TPU v7x, 256 devices: a 4x2x16 block of a 4x16x16 slice. The times are simulated.
256 devices in a mesh: grp: 2 (over y), ep: 32 (over z, core), tp: 4 (over x).
Axes of the slice: x: 4, y: 2, z: 16, core: 2. Of those that a mesh axis runs over, the one named last changes fastest.
The devices are a block of a 4x16x16 slice.
Arguments:
- mixer_tokens: bfloat16 [32768, 2048], P(('grp', 'ep', 'tp')), parts along dimension 0, may hold values from -6 to 6
- mixer_gain: float32 [2048], replicated, may hold values from 0.1 to 1.9
- proj_in: bfloat16 [2048, 1024], P(None, 'tp'), may hold values from -0.125 to 0.125
- pool_weight: bfloat16 [4, 256, 256], P('tp'), may hold values from -0.375 to 0.375
- pool_scale: float32 [1024], P('tp'), may hold values from 0.1 to 1.9
- proj_out: bfloat16 [1024, 2048], P('tp'), may hold values from -0.1875 to 0.1875
- expert_tokens: bfloat16 [32768, 2048], P(('grp', 'ep', 'tp')), parts along dimension 0, may hold values from -6 to 6
- expert_gain: float32 [2048], replicated, may hold values from 0.1 to 1.9
- expert_route: int32 [32768, 2], P(('grp', 'ep')), parts along dimension 0, may hold values from 0 to 63, as said below
- route_gate: float32 [32768, 2], P(('grp', 'ep')), parts along dimension 0, may hold values from 0.1 to 1
- expert_gate: bfloat16 [64, 2048, 1024], P('ep', None, 'tp'), may hold values from -0.125 to 0.125
- expert_up: bfloat16 [64, 2048, 1024], P('ep', None, 'tp'), may hold values from -0.125 to 0.125
- expert_down: bfloat16 [64, 1024, 2048], P('ep', 'tp'), may hold values from -0.1875 to 0.1875
Outputs:
- mixed_rows: bfloat16 [32768, 2048], P(('grp', 'ep', 'tp')), parts along dimension 0
- moe_rows: bfloat16 [32768, 2048], P(('grp', 'ep', 'tp')), parts along dimension 0
There are 2 independent parts, one for each index of `grp`. A program takes and returns all parts, laid end to end along the dimension named above; an argument that names none is the same for every part. Nothing has to cross between parts.
Inputs may be any that keep to these rules, and one draw needn't show every extreme that they name: `expert_route`: each row names two different experts of one group of 4 consecutive experts. In each aligned block of 128 rows (the routes of the tokens that lie on one device) no expert is named by more than 8 rows, and every expert of a group that the block names at all is named by exactly 8 of its rows; one group, the same in every block, is named in every block, and which other groups a block names varies from block to block.
All inputs are finite; a program needn't handle non-finite values.
Results may differ from a plain program's by a relative error of at most 0.011.
Values may be sent and summed in bfloat16 or wider, within the bound.
No kernel may reach another device: no remote copies, remote signals or barrier semaphores. Data moves between devices by JAX's collectives and lax.ppermute only.
A program may use at most 128 MiB of HBM per device.

v0:
```python
import jax
import jax.numpy as jnp
from jax import lax
from jax.sharding import PartitionSpec as P

GROUP_SIZE = 4


norm_eps = 1e-05
rim_rows = 15


def shifted(value, axis, by):
    peers = lax.axis_size(axis)
    pairs = [(i, i + by) for i in range(peers) if 0 <= i + by < peers]
    return lax.ppermute(value, axis, pairs)


def copy_for_each(value, axis):
    peers = lax.axis_size(axis)
    return lax.all_to_all(
        jnp.broadcast_to(value[None], (peers, *value.shape)), axis, 0, 0, tiled=True
    )


def joined_along(blocks, dim):
    blocks = jnp.moveaxis(blocks, 0, dim)
    shape = blocks.shape
    return blocks.reshape(*shape[:dim], shape[dim] * shape[dim + 1], *shape[dim + 2 :])


def gather_directly(value, axis, dim):
    blocks = copy_for_each(value, axis)
    return joined_along(blocks, dim)


def split_up(value, dim, peers):
    before, after = (value.shape[:dim], value.shape[dim + 1 :])
    return jnp.moveaxis(value.reshape(*before, peers, -1, *after), dim, 0)


def sum_at_owner(value, axis, dim):
    blocks = split_up(value, dim, lax.axis_size(axis))
    arrived = lax.all_to_all(blocks, axis, split_axis=0, concat_axis=0, tiled=True)
    return arrived.astype(jnp.float32).sum(axis=0)


def grouped_exchange(value, axis, split_dim, concat_dim, work, item_dim, out_dim):
    items = jax.tree.leaves(value)[0].shape[item_dim]
    count = 2 if items % 2 == 0 else 1
    gathered = []
    for k in range(count):
        group = jax.tree.map(
            lambda a: lax.slice_in_dim(
                a, k * (items // count), (k + 1) * (items // count), axis=item_dim
            ),
            value,
        )
        gathered.append(
            work(
                lax.all_to_all(
                    group, axis, split_axis=split_dim, concat_axis=concat_dim, tiled=True
                )
            )
        )
    return jax.tree.map(lambda *parts: jnp.concatenate(parts, axis=out_dim), *gathered)


def layer_norm(values, norm_gain):
    widened = values.astype(jnp.float32)
    center = jnp.mean(widened, axis=-1, keepdims=True)
    spread = jnp.mean(jnp.square(widened - center), axis=-1, keepdims=True)
    return ((widened - center) * lax.rsqrt(spread + norm_eps) * norm_gain).astype(jnp.bfloat16)


def pooled_diff(extended, windows, first_row):
    widened = extended.astype(jnp.float32)
    row_total = widened.shape[0] - rim_rows
    own_rows = widened[rim_rows:]
    window_sum = own_rows
    for offset in range(1, rim_rows + 1):
        lagged = widened[rim_rows - offset : rim_rows - offset + row_total]
        window_sum = window_sum + jnp.where(offset < windows[None, :], lagged, 0.0)
    position = first_row + jnp.arange(row_total, dtype=jnp.int32)
    covered = jnp.minimum(position[:, None] + 1, windows[None, :]).astype(jnp.float32)
    return (window_sum / covered - own_rows).astype(jnp.bfloat16)


def pool_mix(projected, pool_weight, pool_scale, windows, first_row):
    prior = shifted(projected[-rim_rows:], "ep", 1)
    differences = pooled_diff(jnp.concatenate([prior, projected], axis=0), windows, first_row)
    row_total, local_width = differences.shape
    grouped = differences.reshape(row_total, pool_weight.shape[0], pool_weight.shape[1])
    mixed_groups = jnp.einsum(
        "tgc,gcd->tgd", grouped, pool_weight, preferred_element_type=jnp.float32
    )
    return (mixed_groups.reshape(row_total, local_width) * pool_scale).astype(jnp.bfloat16)


def route_table(routes, experts, capacity):
    flat_route = routes.reshape(-1)
    onehot = (flat_route[:, None] == jnp.arange(experts, dtype=jnp.int32)[None, :]).astype(
        jnp.int32
    )
    earlier = jnp.cumsum(onehot, axis=0) - onehot
    rank_in = jnp.sum(earlier * onehot, axis=1)
    placed = flat_route * capacity + rank_in
    token_mark = jnp.arange(flat_route.shape[0], dtype=jnp.int32) // 2 + 1
    sender = jnp.zeros((experts * capacity,), jnp.int32).at[placed].set(token_mark)
    return (placed, sender)


def fill_slots(rows_here, sender):
    picked = rows_here[jnp.maximum(sender - 1, 0)]
    return jnp.where((sender > 0)[:, None], picked, jnp.zeros_like(picked))


def lift_rows(slot_rows, expert_gate, expert_up):
    gate_part = jnp.einsum(
        "pesd,edh->pesh", slot_rows, expert_gate, preferred_element_type=jnp.float32
    )
    up_part = jnp.einsum("pesd,edh->pesh", slot_rows, expert_up, preferred_element_type=jnp.float32)
    return (jax.nn.silu(gate_part) * up_part).astype(jnp.bfloat16)


def lower_rows(hidden, expert_down):
    return jnp.einsum("pesh,ehd->pesd", hidden, expert_down, preferred_element_type=jnp.float32)


def shards(
    mixer_tokens,
    mixer_gain,
    proj_in,
    pool_weight,
    pool_scale,
    proj_out,
    expert_tokens,
    expert_gain,
    expert_route,
    route_gate,
    expert_gate,
    expert_up,
    expert_down,
):
    ep_count = lax.axis_size("ep")
    tp_index = lax.axis_index("tp")
    ep_index = lax.axis_index("ep")
    own_count = mixer_tokens.shape[0]
    model_width = mixer_tokens.shape[1]
    local_width = proj_in.shape[1]
    group_width = pool_weight.shape[1]
    experts = expert_gate.shape[0] * ep_count
    capacity = own_count * GROUP_SIZE // experts
    channel = tp_index * local_width + jnp.arange(local_width, dtype=jnp.int32)
    windows = jnp.left_shift(jnp.full_like(channel, 2), channel // group_width)
    normed_mixer = layer_norm(mixer_tokens, mixer_gain)
    normed_expert = layer_norm(expert_tokens, expert_gain)
    own_start = tp_index * own_count
    own_gates = lax.dynamic_slice_in_dim(route_gate, own_start, own_count, 0)
    projected = jnp.dot(
        gather_directly(normed_mixer, "tp", 0), proj_in, preferred_element_type=jnp.float32
    ).astype(jnp.bfloat16)
    shard_count = projected.shape[0]
    pooled = pool_mix(projected, pool_weight, pool_scale, windows, ep_index * shard_count)
    mixed_rows = sum_at_owner(
        jnp.dot(pooled, proj_out, preferred_element_type=jnp.float32).astype(jnp.bfloat16), "tp", 0
    ).astype(jnp.bfloat16)
    own_route = lax.dynamic_slice_in_dim(expert_route, own_start, own_count, 0)
    placed, sender = route_table(own_route, experts, capacity)
    outgoing = fill_slots(normed_expert, sender).reshape(ep_count, -1, capacity, model_width)

    def expert_late(arrived):
        hidden = lift_rows(
            lax.all_gather(arrived, "tp", axis=0, tiled=True), expert_gate, expert_up
        )
        summed = lax.psum_scatter(
            lower_rows(hidden, expert_down).astype(jnp.bfloat16),
            "tp",
            scatter_dimension=0,
            tiled=True,
        )
        return lax.all_to_all(summed, "ep", split_axis=0, concat_axis=0, tiled=True)

    returned = grouped_exchange(outgoing, "ep", 0, 0, expert_late, 2, 2)
    expert_out = returned.reshape(-1, model_width)[placed].reshape(own_count, 2, model_width)
    moe_rows = jnp.sum(own_gates[:, :, None] * expert_out.astype(jnp.float32), axis=1).astype(
        jnp.bfloat16
    )
    return (mixed_rows, moe_rows)


def solution(mesh):
    return jax.shard_map(
        shards,
        mesh=mesh,
        in_specs=(
            P(("grp", "ep", "tp"), None),
            P(),
            P(None, "tp"),
            P("tp", None, None),
            P("tp"),
            P("tp", None),
            P(("grp", "ep", "tp"), None),
            P(),
            P(("grp", "ep"), None),
            P(("grp", "ep"), None),
            P("ep", None, "tp"),
            P("ep", None, "tp"),
            P("ep", "tp", None),
        ),
        out_specs=(P(("grp", "ep", "tp"), None), P(("grp", "ep", "tp"), None)),
        check_vma=False,
    )
```

profile of v0, /device:TPU:40, one launch (start us, length us, event | category | flops | bytes accessed | tf_op | source)
XLA Modules:
  0.0 464.9 jit_solution(8590155266023501591)
XLA Ops:
  7.3 0.9 broadcast_multiply_fusion
  8.3 0.1 eq.29
  8.4 0.1 eq.25
  8.6 0.6 reduce-window.6
  9.2 0.2 slice_reduce_fusion
  9.5 0.1 mul.101
  9.8 1.4 scatter_custom_fusion
  11.2 1.2 convert_reduce_fusion
  12.4 1.3 fusion.39
  13.9 1.1 fusion.41
  15.0 3.3 gather_fusion
  18.3 1.8 broadcast_select_fusion
  20.1 1.2 fusion.116
  21.3 79.8 %all_to_all.30 = bf16[32,2,4,2048]{3,2,1,0:T(4,128)(2,1)S(1)} all-to-all(bf16[32,2,4,2048]{3,2,1,0:T(4,128)(2,1)S(1)} %get-tuple-element.4), channel_id=1, replica_groups=mesh['grp'=2,'ep'=32,'tp'=4] {'ep'}, dimensions={0} | all-to-all | bytes 2097152 | tf_op jit(solution)/shard_map/all_to_all | solution.py:61
  101.1 1.6 copy.29
  102.9 59.6 %all_to_all.31 = bf16[32,2,4,2048]{3,2,1,0:T(4,128)(2,1)S(1)} all-to-all(bf16[32,2,4,2048]{3,2,1,0:T(4,128)(2,1)S(1)} %get-tuple-element.5), channel_id=1, replica_groups=mesh['grp'=2,'ep'=32,'tp'=4] {'ep'}, dimensions={0} | all-to-all | bytes 2097152 | tf_op jit(solution)/shard_map/all_to_all | solution.py:61
  162.5 1.6 copy.31
  164.3 4.1 fusion.10
  168.4 7.5 %convert_bitcast_fusion.1 = bf16[128,2,4,2048]{3,0,2,1:T(8,128)(2,1)} fusion(bf16[2,256,2048]{2,1,0:T(8,128)(2,1)S(1)} %copy-done, bf16[128,2,4,2048]{3,0,2,1:T(8,128)(2,1)} %all-gather.3.cloned.1.call-done, bf16[2,2048,256]{2,1,0:T(8,128)(2,1)} %param.24, f32[128,2,4,256]{3,0,2,1:T(8,128)S(1)} %fusion.10), kind=kOutput, calls=%fused_computation.4 | convolution fusion | flops 2151153664 | bytes 13631488 | tf_op jit(solution)/shard_map/pesh,ehd->pesd/dot_general | solution.py:127
  176.0 1.0 copy-done.2
  176.9 0.2 convert_reduce_fusion.1
  177.1 0.3 fusion.42
  177.4 0.4 fusion.44
  177.8 1.6 broadcast_in_dim.150
  179.3 4.7 %all-to-all-start = ((bf16[4,128,2048]{2,1,0:T(8,128)(2,1)}), bf16[4,128,2048]{2,1,0:T(8,128)(2,1)}, u32[]{:S(2)}, u32[]{:S(2)}) async-start(bf16[4,128,2048]{2,1,0:T(8,128)(2,1)} %broadcast_in_dim.150), calls=%async_computation | async-start | bytes 4194304 | tf_op jit(solution)/shard_map/all_to_all | solution.py:21
  184.1 47.5 %all-gather.5.cloned.1.call-done = bf16[128,2,4,2048]{3,0,2,1:T(8,128)(2,1)} async-done(((bf16[32,2,4,2048]{3,0,2,1:T(8,128)(2,1)}), bf16[128,2,4,2048]{3,0,2,1:T(8,128)(2,1)}) %all-gather.5.cloned.1.call-update) | async-done | bytes 4194320 | tf_op jit(solution)/shard_map/all_gather | solution.py:174
  231.7 4.1 fusion.13
  235.8 7.3 %convert_bitcast_fusion = bf16[128,2,4,2048]{3,0,2,1:T(8,128)(2,1)} fusion(bf16[2,256,2048]{2,1,0:T(8,128)(2,1)S(1)} %copy-done, bf16[128,2,4,2048]{3,0,2,1:T(8,128)(2,1)} %all-gather.5.cloned.1.call-done, bf16[2,2048,256]{2,1,0:T(8,128)(2,1)} %param.24, f32[128,2,4,256]{3,0,2,1:T(8,128)S(1)} %fusion.13), kind=kOutput, calls=%fused_computation.3 | convolution fusion | flops 2151153664 | bytes 13631488 | tf_op jit(solution)/shard_map/pesh,ehd->pesd/dot_general | solution.py:127
  243.4 2.6 convolution_convert_fusion.1
  246.0 1.3 collective-permute-start
  247.4 0.8 collective-permute-done
  248.2 4.9 %convolution_convert_fusion = bf16[512,2048]{1,0:T(8,128)(2,1)} fusion(bf16[256,2048]{1,0:T(8,128)(2,1)} %param.18, f32[256]{0:T(256)S(1)} %copy-done.5, f32[527,256]{1,0:T(8,128)S(1)} %maximum_convert_fusion, s32[256]{0:T(256)S(1)} %fusion.111, s32[512]{0:T(512)S(1)} %add_add_fusion, pred[256]{0:T(512)(128)(4,1)S(1)} %get-tuple-element.6, ...), kind=kOutput, calls=%fused_computation.5 | convolution fusion | flops 609878016 | bytes 11677184 | tf_op jit(solution)/shard_map/dot_general | solution.py:166
  253.1 4.6 all-to-all-start.1
  257.7 53.1 %reduce-scatter.3.cloned.1.call-done = bf16[32,2,4,2048]{3,0,2,1:T(8,128)(2,1)} async-done(((bf16[128,2,4,2048]{3,0,2,1:T(8,128)(2,1)}), bf16[32,2,4,2048]{3,0,2,1:T(8,128)(2,1)}) %reduce-scatter.3.cloned.1.call-update) | async-done | bytes 1048592 | tf_op jit(solution)/shard_map/reduce_scatter | solution.py:176
  310.8 3.0 copy.30
  313.8 12.1 %all-to-all-start.3 = ((bf16[32,2,4,2048]{3,2,1,0:T(4,128)(2,1)}), bf16[32,2,4,2048]{3,2,1,0:T(4,128)(2,1)S(1)}, u32[]{:S(2)}, u32[]{:S(2)}) async-start(bf16[32,2,4,2048]{3,2,1,0:T(4,128)(2,1)} %copy.30), calls=%async_computation.4 | async-start | bytes 2097152 | tf_op jit(solution)/shard_map/all_to_all | solution.py:182
  326.0 39.4 %reduce-scatter.5.cloned.1.call-done = bf16[32,2,4,2048]{3,0,2,1:T(8,128)(2,1)} async-done(((bf16[128,2,4,2048]{3,0,2,1:T(8,128)(2,1)}), bf16[32,2,4,2048]{3,0,2,1:T(8,128)(2,1)}) %reduce-scatter.5.cloned.1.call-update) | async-done | bytes 1048592 | tf_op jit(solution)/shard_map/reduce_scatter | solution.py:176
  365.3 3.1 copy.32
  368.4 12.8 %all-to-all-done.3 = bf16[32,2,4,2048]{3,2,1,0:T(4,128)(2,1)S(1)} async-done(((bf16[32,2,4,2048]{3,2,1,0:T(4,128)(2,1)}), bf16[32,2,4,2048]{3,2,1,0:T(4,128)(2,1)S(1)}, u32[]{:S(2)}, u32[]{:S(2)}) %all-to-all-start.3) | async-done | bytes 1048608 | tf_op jit(solution)/shard_map/all_to_all | solution.py:182
  381.3 5.7 %all-to-all-start.5 = ((bf16[32,2,4,2048]{3,2,1,0:T(4,128)(2,1)}), bf16[32,2,4,2048]{3,2,1,0:T(4,128)(2,1)}, u32[]{:S(2)}, u32[]{:S(2)}) async-start(bf16[32,2,4,2048]{3,2,1,0:T(4,128)(2,1)} %copy.32), calls=%async_computation.7 | async-start | bytes 2097152 | tf_op jit(solution)/shard_map/all_to_all | solution.py:182
  386.9 0.7 constant_dynamic-slice_fusion.1
  387.6 0.1 copy.24
  387.8 2.9 reduce_sum.70
  390.7 51.8 %all-to-all-done.5 = bf16[32,2,4,2048]{3,2,1,0:T(4,128)(2,1)} async-done(((bf16[32,2,4,2048]{3,2,1,0:T(4,128)(2,1)}), bf16[32,2,4,2048]{3,2,1,0:T(4,128)(2,1)}, u32[]{:S(2)}, u32[]{:S(2)}) %all-to-all-start.5) | async-done | bytes 1048608 | tf_op jit(solution)/shard_map/all_to_all | solution.py:182
  442.5 3.6 pad_maximum_fusion
  446.2 4.2 gather_fusion.1
  450.4 2.4 reshape.198
  452.8 5.6 %multiply_reduce_fusion = bf16[128,2048]{1,0:T(8,128)(2,1)} fusion(f32[128,2,2048]{2,1,0:T(2,128)} %reshape.198, f32[128,2]{1,0:T(8,128)S(1)} %copy.24), kind=kLoop, calls=%fused_computation.17 | loop fusion | flops 786432 | bytes 2622464 | tf_op jit(solution)/shard_map/reduce_sum | solution.py:186
  (51 shorter events, 1.3 us)
Async XLA Ops:
  7.2 161.2 %copy-start = (bf16[2,256,2048]{2,1,0:T(8,128)(2,1)S(1)}, bf16[2,256,2048]{2,1,0:T(8,128)(2,1)}, u32[]{:S(2)}) copy-start(bf16[2,256,2048]{2,1,0:T(8,128)(2,1)} %param.25) | copy-start | bytes 6291460
  7.2 6.7 %copy-start.1 = (bf16[128,2048]{1,0:T(8,128)(2,1)S(1)}, bf16[128,2048]{1,0:T(8,128)(2,1)}, u32[]{:S(2)}) copy-start(bf16[128,2048]{1,0:T(8,128)(2,1)} %param.19) | copy-start | bytes 1572868
  7.2 157.0 %all-gather.3.cloned.1.call-start = ((), (), s32[]{:S(2)}) async-start(), calls=%async_computation.8 | async-start | bytes 5242880 | tf_op jit(solution)/shard_map/all_gather | solution.py:174
  102.8 128.9 %all-gather.5.cloned.1.call-start = ((), (), s32[]{:S(2)}) async-start(), calls=%async_computation.10 | async-start | bytes 5242880 | tf_op jit(solution)/shard_map/all_gather | solution.py:174
  164.2 146.6 %reduce-scatter.3.cloned.1.call-start = ((), (), s32[]{:S(2)}) async-start(), calls=%async_computation.9 | async-start | bytes 5242880 | tf_op jit(solution)/shard_map/reduce_scatter | solution.py:176
  175.9 1.0 copy-start.2
  175.9 1.5 copy-start.3
  179.3 64.0 %all-to-all-start = ((bf16[4,128,2048]{2,1,0:T(8,128)(2,1)}), bf16[4,128,2048]{2,1,0:T(8,128)(2,1)}, u32[]{:S(2)}, u32[]{:S(2)}) async-start(bf16[4,128,2048]{2,1,0:T(8,128)(2,1)} %broadcast_in_dim.150), calls=%async_computation | async-start | bytes 4194304 | tf_op jit(solution)/shard_map/all_to_all | solution.py:21
  184.1 181.3 %reduce-scatter.5.cloned.1.call-start = ((), (), s32[]{:S(2)}) async-start(), calls=%async_computation.11 | async-start | bytes 5242880 | tf_op jit(solution)/shard_map/reduce_scatter | solution.py:176
  243.4 4.8 %copy-start.4 = (bf16[1,256,256]{2,1,0:T(8,128)(2,1)S(1)}, bf16[1,256,256]{2,1,0:T(8,128)(2,1)}, u32[]{:S(2)}) copy-start(bf16[1,256,256]{2,1,0:T(8,128)(2,1)} %param.16) | copy-start | bytes 393220
  243.4 4.8 %copy-start.5 = (f32[256]{0:T(256)S(1)}, f32[256]{0:T(256)}, u32[]{:S(2)}) copy-start(f32[256]{0:T(256)} %param.17) | copy-start | bytes 3076
  246.0 2.1 collective-permute-start
  253.1 60.7 %all-to-all-start.1 = ((bf16[4,128,2048]{2,1,0:T(8,128)(2,1)}), bf16[4,128,2048]{2,1,0:T(8,128)(2,1)}, u32[]{:S(2)}, u32[]{:S(2)}) async-start(bf16[4,128,2048]{2,1,0:T(8,128)(2,1)} %bitcast.103), calls=%async_computation.1 | async-start | bytes 4194304 | tf_op jit(solution)/shard_map/all_to_all | solution.py:44
  313.8 67.4 %all-to-all-start.3 = ((bf16[32,2,4,2048]{3,2,1,0:T(4,128)(2,1)}), bf16[32,2,4,2048]{3,2,1,0:T(4,128)(2,1)S(1)}, u32[]{:S(2)}, u32[]{:S(2)}) async-start(bf16[32,2,4,2048]{3,2,1,0:T(4,128)(2,1)} %copy.30), calls=%async_computation.4 | async-start | bytes 2097152 | tf_op jit(solution)/shard_map/all_to_all | solution.py:182
  381.3 61.3 %all-to-all-start.5 = ((bf16[32,2,4,2048]{3,2,1,0:T(4,128)(2,1)}), bf16[32,2,4,2048]{3,2,1,0:T(4,128)(2,1)}, u32[]{:S(2)}, u32[]{:S(2)}) async-start(bf16[32,2,4,2048]{3,2,1,0:T(4,128)(2,1)} %copy.32), calls=%async_computation.7 | async-start | bytes 2097152 | tf_op jit(solution)/shard_map/all_to_all | solution.py:182
Sparse Core Ops, SparseCore 0:
  102.9 46.3 all-gather.2
  164.3 67.3 all-gather.4
  234.2 76.5 reduce-scatter.2
  313.2 52.0 reduce-scatter.4
where the time goes:
time: 467 us; the launch traced here: 465 us
  waiting for transfers between devices  206 us (44%)
  blocking collectives  139 us (30%)
  matrix products  30.6 us (7%)
  starting transfers between devices  28.6 us (6%)
  local copies, waits for them, and re-layouts  26.1 us (6%)
  other arithmetic  20.2 us (4%)
  between operations  14.1 us (3%)
    all_to_all x2, blocking collectives, grouped_exchange(): lax.all_to_all(group, axis, split_axis=split_dim, concat_axis=concat_dim,...  139 us
    reduce_scatter x2, waiting for transfers between devices, expert_late(): lax.psum_scatter(lower_rows(hidden, expert_down).astype(jnp.bfloat16), 't...  92.5 us
    all_to_all x2, waiting for transfers between devices, expert_late(): return lax.all_to_all(summed, 'ep', split_axis=0, concat_axis=0, tiled=True)  64.7 us
    all_gather x2, waiting for transfers between devices, expert_late(): lax.all_gather(arrived, 'tp', axis=0, tiled=True)  47.6 us
    all_to_all x2, starting transfers between devices, expert_late(): return lax.all_to_all(summed, 'ep', split_axis=0, concat_axis=0, tiled=True)  17.8 us
    dot_general x2, matrix products, lower_rows(): jnp.einsum('pesh,ehd->pesd', hidden, expert_down, preferred_element_type=...  14.8 us
  transfers between devices with their start and end apart: 9, of which 6 were waited for; matrix products, arithmetic and copies ran while one was open for 10% of the time, Pallas kernels for 0%

commit v1 on v0

v1 whole, which is shorter than its diff:
```python
import jax
import jax.numpy as jnp
from jax import lax
from jax.sharding import PartitionSpec as P

GROUP_SIZE = 4


norm_eps = 1e-05
rim_rows = 15
chunks = 2


def shifted(value, axis, by):
    peers = lax.axis_size(axis)
    pairs = [(i, i + by) for i in range(peers) if 0 <= i + by < peers]
    return lax.ppermute(value, axis, pairs)


def copy_for_each(value, axis):
    peers = lax.axis_size(axis)
    return lax.all_to_all(
        jnp.broadcast_to(value[None], (peers, *value.shape)), axis, 0, 0, tiled=True
    )


def sum_at_owner(value, axis):
    peers = lax.axis_size(axis)
    blocks = value.reshape(peers, -1, value.shape[1])
    arrived = lax.all_to_all(blocks, axis, split_axis=0, concat_axis=0, tiled=True)
    return arrived.astype(jnp.float32).sum(axis=0)


def layer_norm(values, norm_gain):
    widened = values.astype(jnp.float32)
    center = jnp.mean(widened, axis=-1, keepdims=True)
    spread = jnp.mean(jnp.square(widened - center), axis=-1, keepdims=True)
    return ((widened - center) * lax.rsqrt(spread + norm_eps) * norm_gain).astype(jnp.bfloat16)


def pooled_diff(extended, windows, first_row):
    widened = extended.astype(jnp.float32)
    row_total = widened.shape[0] - rim_rows
    own_rows = widened[rim_rows:]
    window_sum = own_rows
    for offset in range(1, rim_rows + 1):
        lagged = widened[rim_rows - offset : rim_rows - offset + row_total]
        window_sum = window_sum + jnp.where(offset < windows[None, :], lagged, 0.0)
    position = first_row + jnp.arange(row_total, dtype=jnp.int32)
    covered = jnp.minimum(position[:, None] + 1, windows[None, :]).astype(jnp.float32)
    return (window_sum / covered - own_rows).astype(jnp.bfloat16)


def pool_mix(projected, pool_weight, pool_scale, windows, first_row):
    prior = shifted(projected[-rim_rows:], "ep", 1)
    differences = pooled_diff(jnp.concatenate([prior, projected], axis=0), windows, first_row)
    row_total, local_width = differences.shape
    grouped = differences.reshape(row_total, pool_weight.shape[0], pool_weight.shape[1])
    mixed_groups = jnp.einsum(
        "tgc,gcd->tgd", grouped, pool_weight, preferred_element_type=jnp.float32
    )
    return (mixed_groups.reshape(row_total, local_width) * pool_scale).astype(jnp.bfloat16)


def route_slots(routes, groups, packet):
    rows = routes.shape[1]
    group = routes[:, :, 0] // GROUP_SIZE
    named = group[:, :, None] == jnp.arange(groups, dtype=jnp.int32)
    order = jnp.arange(rows, dtype=jnp.int32)
    before = (order[:, None] > order[None, :]).astype(jnp.bfloat16)
    earlier = jnp.einsum(
        "tu,bug->btg", before, named.astype(jnp.bfloat16), preferred_element_type=jnp.float32
    )
    rank = jnp.sum(jnp.where(named, earlier, 0.0), axis=2).astype(jnp.int32)
    return group * packet + rank


def same_core(value, peers_per_group):
    peers = lax.axis_size("ep")
    rings = [list(range(c, peers, peers_per_group)) for c in range(peers_per_group)]
    return lax.all_to_all(value, "ep", 0, 0, axis_index_groups=rings, tiled=True)


def expert_rows(rows, weights, sets):
    total = None
    for (gate, up, down), weight in zip(sets, weights):
        parts = []
        for e in range(gate.shape[0]):
            gate_part = jnp.dot(rows, gate[e], preferred_element_type=jnp.float32)
            up_part = jnp.dot(rows, up[e], preferred_element_type=jnp.float32)
            parts.append(
                (jax.nn.silu(gate_part) * up_part * weight[:, e : e + 1]).astype(jnp.bfloat16)
            )
        hidden = jnp.concatenate(parts, axis=1)
        part = jnp.dot(
            hidden, down.reshape(-1, down.shape[2]), preferred_element_type=jnp.float32
        )
        total = part if total is None else total + part
    return total.astype(jnp.bfloat16)


def shards(
    mixer_tokens,
    mixer_gain,
    proj_in,
    pool_weight,
    pool_scale,
    proj_out,
    expert_tokens,
    expert_gain,
    expert_route,
    route_gate,
    expert_gate,
    expert_up,
    expert_down,
):
    ep_count = lax.axis_size("ep")
    tp_count = lax.axis_size("tp")
    tp_index = lax.axis_index("tp")
    ep_index = lax.axis_index("ep")
    own_count, model_width = mixer_tokens.shape
    local_width = proj_in.shape[1]
    group_width = pool_weight.shape[1]
    local_experts = expert_gate.shape[0]
    experts = local_experts * ep_count
    capacity = own_count * GROUP_SIZE // experts
    packet = capacity * GROUP_SIZE // 2
    groups = experts // GROUP_SIZE
    holders = GROUP_SIZE // local_experts
    place = ep_index % holders

    blocks = expert_route.reshape(tp_count, own_count, 2)
    slots = route_slots(blocks, groups, packet)
    member = blocks % GROUP_SIZE
    local = jnp.arange(GROUP_SIZE, dtype=jnp.int32)
    gates = route_gate.reshape(tp_count, own_count, 2)
    by_member = jnp.sum(
        jnp.where(member[:, :, :, None] == local, gates[:, :, :, None], 0.0), axis=2
    )
    slot_range = jnp.arange(groups * packet, dtype=jnp.int32)
    placed = slots[:, :, None] == slot_range
    slot_weight = jnp.einsum(
        "btj,bts->bjs",
        by_member,
        placed.astype(jnp.float32),
        precision=lax.Precision.HIGHEST,
        preferred_element_type=jnp.float32,
    )
    slot_weight = slot_weight.reshape(tp_count, GROUP_SIZE, groups, packet)
    slot_weight = slot_weight.transpose(2, 0, 1, 3).reshape(groups, -1)
    weights = same_core(slot_weight, holders).reshape(groups, tp_count, GROUP_SIZE, packet)
    weights = weights.transpose(1, 0, 3, 2)

    own_slots = lax.dynamic_index_in_dim(slots, tp_index, 0, keepdims=False)
    pick = (own_slots[:, None] == slot_range).astype(jnp.bfloat16)
    normed_expert = layer_norm(expert_tokens, expert_gain)
    outgoing = jnp.einsum(
        "ts,td->sd", pick, normed_expert, preferred_element_type=jnp.float32
    ).astype(jnp.bfloat16)
    outgoing = outgoing.reshape(groups, packet, model_width)

    own_set = (expert_gate, expert_up, expert_down)
    sets = [own_set]
    for s in range(1, holders):
        pairs = [(i, i - i % holders + (i + s) % holders) for i in range(ep_count)]
        sets.append(tuple(lax.ppermute(w, "ep", pairs) for w in own_set))

    normed_mixer = layer_norm(mixer_tokens, mixer_gain)
    channel = tp_index * local_width + jnp.arange(local_width, dtype=jnp.int32)
    windows = jnp.left_shift(jnp.full_like(channel, 2), channel // group_width)
    gathered = copy_for_each(normed_mixer, "tp").reshape(-1, model_width)
    projected = jnp.dot(gathered, proj_in, preferred_element_type=jnp.float32).astype(
        jnp.bfloat16
    )
    pooled = pool_mix(
        projected, pool_weight, pool_scale, windows, ep_index * projected.shape[0]
    )
    mixed_rows = sum_at_owner(
        jnp.dot(pooled, proj_out, preferred_element_type=jnp.float32).astype(jnp.bfloat16), "tp"
    ).astype(jnp.bfloat16)

    step = packet // chunks
    back = []
    for k in range(chunks):
        sent = outgoing[:, k * step : (k + 1) * step]
        arrived = same_core(sent, holders)
        rows = lax.all_gather(arrived, "tp", axis=0, tiled=False).reshape(-1, model_width)
        weight = weights[:, :, k * step : (k + 1) * step].reshape(-1, GROUP_SIZE)
        by_set = [
            lax.dynamic_slice_in_dim(
                weight, (place - s) % holders * local_experts, local_experts, 1
            )
            for s in range(holders)
        ]
        partial = expert_rows(rows, by_set, sets)
        summed = lax.psum_scatter(
            partial.reshape(tp_count, -1, model_width), "tp", scatter_dimension=0, tiled=True
        )
        back.append(same_core(summed.reshape(groups, step, model_width), holders))
    total = None
    pick_parts = pick.reshape(own_count, groups, packet)
    for k in range(chunks):
        part = jnp.dot(
            pick_parts[:, :, k * step : (k + 1) * step].reshape(own_count, -1),
            back[k].reshape(-1, model_width),
            preferred_element_type=jnp.float32,
        )
        total = part if total is None else total + part
    return (mixed_rows, total.astype(jnp.bfloat16))


def solution(mesh):
    return jax.shard_map(
        shards,
        mesh=mesh,
        in_specs=(
            P(("grp", "ep", "tp"), None),
            P(),
            P(None, "tp"),
            P("tp", None, None),
            P("tp"),
            P("tp", None),
            P(("grp", "ep", "tp"), None),
            P(),
            P(("grp", "ep"), None),
            P(("grp", "ep"), None),
            P("ep", None, "tp"),
            P("ep", None, "tp"),
            P("ep", "tp", None),
        ),
        out_specs=(P(("grp", "ep", "tp"), None), P(("grp", "ep", "tp"), None)),
        check_vma=False,
    )
```

time: 467 us -> 311 us (0.67)
  waiting for transfers between devices: 206 us -> 101 us
  blocking collectives: 139 us -> 87.1 us
  matrix products: 30.6 us -> 53.8 us
  local copies, waits for them, and re-layouts: 26.1 us -> 6.52 us
  other arithmetic: 20.2 us -> 9 us
  starting transfers between devices: 28.6 us -> 37.4 us
    reduce_scatter x2, waiting for transfers between devices: 92.5 us -> 11.7 us  [shards(): lax.psum_scatter(partial.reshape(tp_count, -1, model_width), 'tp', scatte...]
    all_to_all x2, blocking collectives: 139 us -> 87.1 us  [the longest x1 52.9 us: same_core(): lax.all_to_all(value, 'ep', 0, 0, axis_index_groups=rings, tiled=True)]
    all_gather x2, waiting for transfers between devices: 47.6 us -> 9.7 us  [shards(): lax.all_gather(arrived, 'tp', axis=0, tiled=False).reshape(-1, model_width)]
    dot_general x5 -> x26, matrix products: 25.7 us -> 50.2 us  [the longest x8 18.7 us: expert_rows(): gate_part = jnp.dot(rows, gate[e], preferred_element_type=jnp.float32)]
    all_to_all x3 -> x4, waiting for transfers between devices: 64.7 us -> 76.4 us  [same_core(): lax.all_to_all(value, 'ep', 0, 0, axis_index_groups=rings, tiled=True)]
    all_to_all x3 -> x4, starting transfers between devices: 22.4 us -> 30.1 us  [same_core(): lax.all_to_all(value, 'ep', 0, 0, axis_index_groups=rings, tiled=True)]
    gather x2 -> x0, local copies, waits for them, and re-layouts: 7.57 us -> none  [the longest x1 4.22 us: shards(): returned.reshape(-1, model_width)[placed].reshape(own_count, 2, model_width)]
    reduce_scatter x2 -> x0, local copies, waits for them, and re-layouts: 6.1 us -> none  [expert_late(): lax.psum_scatter(lower_rows(hidden, expert_down).astype(jnp.bfloat16), 't...]
  transfers between devices with their start and end apart: 9 -> 13, of which waited for: 6 -> 7; matrix products, arithmetic and copies ran while one was open for 10% -> 19% of each run, Pallas kernels for 0% -> 0%
where the time goes in v1:
time: 311 us; the launch traced here: 309 us
  waiting for transfers between devices  101 us (32%)
  blocking collectives  87.1 us (28%)
  matrix products  53.8 us (17%)
  starting transfers between devices  37.4 us (12%)
  between operations  14.4 us (5%)
  other arithmetic  9 us (3%)
  local copies, waits for them, and re-layouts  6.52 us (2%)
    all_to_all x4, waiting for transfers between devices, same_core(): lax.all_to_all(value, 'ep', 0, 0, axis_index_groups=rings, tiled=True)  76.4 us
    all_to_all x1, blocking collectives, same_core(): lax.all_to_all(value, 'ep', 0, 0, axis_index_groups=rings, tiled=True)  52.9 us
    all_to_all x1, blocking collectives, sum_at_owner(): lax.all_to_all(blocks, axis, split_axis=0, concat_axis=0, tiled=True)  34.2 us
    all_to_all x4, starting transfers between devices, same_core(): lax.all_to_all(value, 'ep', 0, 0, axis_index_groups=rings, tiled=True)  30.1 us
    dot_general x8, matrix products, expert_rows(): gate_part = jnp.dot(rows, gate[e], preferred_element_type=jnp.float32)  18.7 us
    reduce_scatter x2, waiting for transfers between devices, shards(): lax.psum_scatter(partial.reshape(tp_count, -1, model_width), 'tp', scatte...  11.7 us
    dot_general x4, matrix products, expert_rows(): jnp.dot(hidden, down.reshape(-1, down.shape[2]), preferred_element_type=j...  11.6 us
    dot_general x8, matrix products, expert_rows(): up_part = jnp.dot(rows, up[e], preferred_element_type=jnp.float32)  11.3 us
  transfers between devices with their start and end apart: 13, of which 7 were waited for; matrix products, arithmetic and copies ran while one was open for 19% of the time, Pallas kernels for 0%

profile of v1, /device:TPU:40, one launch (start us, length us, event | category | flops | bytes accessed | tf_op | source)
XLA Modules:
  0.0 309.3 jit_solution(16078520964227296294)
XLA Ops:
  7.3 1.3 convert_reduce_fusion
  8.5 1.3 fusion.77
  10.8 1.6 convolution_convert_fusion.1
  12.4 0.9 fusion.202
  13.3 52.9 %all_to_all.40 = bf16[16,8,2048]{2,1,0:T(8,128)(2,1)} all-to-all(bf16[16,8,2048]{2,1,0:T(8,128)(2,1)S(1)} %get-tuple-element.3), channel_id=1, replica_groups={{0,8,16,24,32,40,48,56,64,72,80,88,96,104,112,120},{4,12,20,28,36,44,52..., dimensions={0} | all-to-all | bytes 1048576 | tf_op jit(solution)/shard_map/all_to_all | solution.py:81
  67.6 6.6 %all-to-all-start.3 = ((f32[16,1,256]{2,1,0:T(1,128)}), f32[16,1,256]{2,1,0:T(1,128)S(1)}, u32[]{:S(2)}, u32[]{:S(2)}) async-start(f32[16,1,256]{2,1,0:T(1,128)} %all_to_all.32), calls=%async_computation.3 | async-start | bytes 32768 | tf_op jit(solution)/shard_map/all_to_all | solution.py:81
  75.1 11.5 %all-to-all-done.3 = f32[16,1,256]{2,1,0:T(1,128)S(1)} async-done(((f32[16,1,256]{2,1,0:T(1,128)}), f32[16,1,256]{2,1,0:T(1,128)S(1)}, u32[]{:S(2)}, u32[]{:S(2)}) %all-to-all-start.3) | async-done | bytes 16416 | tf_op jit(solution)/shard_map/all_to_all | solution.py:81
  86.5 4.6 %all-to-all-start.2 = ((bf16[16,8,2048]{2,1,0:T(8,128)(2,1)}), bf16[16,8,2048]{2,1,0:T(8,128)(2,1)}, u32[]{:S(2)}, u32[]{:S(2)}) async-start(bf16[16,8,2048]{2,1,0:T(8,128)(2,1)} %get-tuple-element.2), calls=%async_computation.2 | async-start | bytes 1048576 | tf_op jit(solution)/shard_map/all_to_all | solution.py:81
  91.2 1.2 convert_reduce_fusion.1
  92.4 1.3 fusion.80
  93.8 2.2 fusion.82
  96.7 21.5 %all-to-all-done.2 = bf16[16,8,2048]{2,1,0:T(8,128)(2,1)} async-done(((bf16[16,8,2048]{2,1,0:T(8,128)(2,1)}), bf16[16,8,2048]{2,1,0:T(8,128)(2,1)}, u32[]{:S(2)}, u32[]{:S(2)}) %all-to-all-start.2) | async-done | bytes 524320 | tf_op jit(solution)/shard_map/all_to_all | solution.py:81
  118.2 2.6 broadcast_in_dim.157
  120.8 4.6 %all-to-all-start = ((bf16[4,128,2048]{2,1,0:T(8,128)(2,1)}), bf16[4,128,2048]{2,1,0:T(8,128)(2,1)}, u32[]{:S(2)}, u32[]{:S(2)}) async-start(bf16[4,128,2048]{2,1,0:T(8,128)(2,1)} %broadcast_in_dim.157), calls=%async_computation | async-start | bytes 4194304 | tf_op jit(solution)/shard_map/all_to_all | solution.py:22
  126.5 2.8 fusion.12
  129.3 2.5 fusion.16
  131.9 0.8 fusion.62
  132.7 2.0 fusion.4
  134.7 0.8 fusion.65
  135.5 2.0 multiply_convert_fusion
  137.5 2.0 fusion.8
  139.5 2.1 multiply_convert_fusion.1
  141.6 1.3 fusion.124
  142.9 4.4 %add_convert_fusion = bf16[512,2048]{1,0:T(8,128)(2,1)} fusion(f32[512,2048]{1,0:T(8,128)S(1)} %fusion.124, bf16[512,2048]{1,0:T(8,128)(2,1)} %bitcast.28, bf16[512,256]{0,1:T(8,128)(2,1)S(1)} %multiply_convert_fusion, bf16[512,256]{0,1:T(8,128)(2,1)S(1)} %multiply_convert_fusion.1), kind=kOutput, calls=%fused_computation | convolution fusion | flops 1076887552 | bytes 8912896 | tf_op jit(solution)/shard_map/dot_general | solution.py:95
  147.4 2.4 all-to-all-done
  149.8 2.6 convolution_convert_fusion.2
  152.4 1.5 collective-permute-start
  154.0 9.7 %all-gather.5.cloned.1.call-done = bf16[64,8,2048]{2,1,0:T(8,128)(2,1)} async-done(((bf16[16,8,2048]{2,1,0:T(8,128)(2,1)}), bf16[64,8,2048]{2,1,0:T(8,128)(2,1)}) %all-gather.5.cloned.1.call-update) | async-done | bytes 2097168 | tf_op jit(solution)/shard_map/all_gather | solution.py:187
  163.6 2.8 fusion.28
  166.4 2.5 fusion.32
  168.9 2.0 fusion.20
  171.0 2.1 fusion.24
  173.1 0.8 fusion.68
  173.9 0.8 fusion.71
  174.7 2.0 multiply_convert_fusion.2
  176.7 2.0 multiply_convert_fusion.3
  178.8 1.3 fusion.117
  180.1 4.7 %add_convert_fusion.1 = bf16[512,2048]{1,0:T(8,128)(2,1)} fusion(f32[512,2048]{1,0:T(8,128)S(1)} %fusion.117, bf16[512,2048]{1,0:T(8,128)(2,1)} %bitcast.28, bf16[512,256]{0,1:T(8,128)(2,1)S(1)} %multiply_convert_fusion.2, bf16[512,256]{0,1:T(8,128)(2,1)S(1)} %multiply_convert_fusion.3), kind=kOutput, calls=%fused_computation.1 | convolution fusion | flops 1076887552 | bytes 8912896 | tf_op jit(solution)/shard_map/dot_general | solution.py:95
  185.6 3.7 %convolution_convert_fusion = bf16[512,2048]{1,0:T(8,128)(2,1)} fusion(bf16[256,2048]{1,0:T(8,128)(2,1)S(1)} %copy-done, f32[256]{0:T(256)S(1)} %copy-done.11, f32[527,256]{1,0:T(8,128)S(1)} %maximum_convert_fusion, s32[256]{0:T(256)S(1)} %fusion.193, s32[512]{0:T(512)S(1)} %add_add_fusion, pred[256]{0:T(512)(128)(4,1)S(1)} %get-tuple-element.14, ...), kind=kOutput, calls=%fused_computation.2 | convolution fusion | flops 609878016 | bytes 11677184 | tf_op jit(solution)/shard_map/dot_general | solution.py:179
  189.3 34.2 %all_to_all.41 = bf16[4,128,2048]{2,1,0:T(8,128)(2,1)S(1)} all-to-all(bf16[4,128,2048]{2,1,0:T(8,128)(2,1)} %bitcast.204), channel_id=1, replica_groups=mesh['grp'=2,'ep'=32,'tp'=4] {'tp'}, dimensions={0} | all-to-all | bytes 4194304 | tf_op jit(solution)/shard_map/all_to_all | solution.py:30
  223.5 12.4 %all-to-all-start.6 = ((bf16[16,8,2048]{2,1,0:T(8,128)(2,1)}), bf16[16,8,2048]{2,1,0:T(8,128)(2,1)}, u32[]{:S(2)}, u32[]{:S(2)}) async-start(bf16[16,8,2048]{2,1,0:T(8,128)(2,1)} %bitcast.206), calls=%async_computation.8 | async-start | bytes 1048576 | tf_op jit(solution)/shard_map/all_to_all | solution.py:81
  235.9 11.7 %reduce-scatter.3.cloned.1.call-done = bf16[1,128,2048]{2,1,0:T(8,128)(2,1)} async-done(((bf16[4,128,2048]{2,1,0:T(8,128)(2,1)}), bf16[1,128,2048]{2,1,0:T(8,128)(2,1)}) %reduce-scatter.3.cloned.1.call-update) | async-done | bytes 524304 | tf_op jit(solution)/shard_map/reduce_scatter | solution.py:196
  247.5 17.3 %all-to-all-done.6 = bf16[16,8,2048]{2,1,0:T(8,128)(2,1)} async-done(((bf16[16,8,2048]{2,1,0:T(8,128)(2,1)}), bf16[16,8,2048]{2,1,0:T(8,128)(2,1)}, u32[]{:S(2)}, u32[]{:S(2)}) %all-to-all-start.6) | async-done | bytes 524320 | tf_op jit(solution)/shard_map/all_to_all | solution.py:81
  264.8 6.5 %all-to-all-start.4 = ((bf16[16,8,2048]{2,1,0:T(8,128)(2,1)}), bf16[16,8,2048]{2,1,0:T(8,128)(2,1)}, u32[]{:S(2)}, u32[]{:S(2)}) async-start(bf16[16,8,2048]{2,1,0:T(8,128)(2,1)} %bitcast.207), calls=%async_computation.5 | async-start | bytes 1048576 | tf_op jit(solution)/shard_map/all_to_all | solution.py:81
  271.4 1.3 reduce_sum.68
  272.7 1.6 convolution_bitcast_fusion
  274.3 26.1 %all-to-all-done.4 = bf16[16,8,2048]{2,1,0:T(8,128)(2,1)} async-done(((bf16[16,8,2048]{2,1,0:T(8,128)(2,1)}), bf16[16,8,2048]{2,1,0:T(8,128)(2,1)}, u32[]{:S(2)}, u32[]{:S(2)}) %all-to-all-start.4) | async-done | bytes 524320 | tf_op jit(solution)/shard_map/all_to_all | solution.py:81
  300.4 2.4 fusion.1
  (78 shorter events, 5.9 us)
Async XLA Ops:
  7.2 177.7 %copy-start = (bf16[256,2048]{1,0:T(8,128)(2,1)S(1)}, bf16[256,2048]{1,0:T(8,128)(2,1)}, u32[]{:S(2)}) copy-start(bf16[256,2048]{1,0:T(8,128)(2,1)} %param.18) | copy-start | bytes 3145732
  7.2 119.3 %all-gather.7.cloned.1.call-start = ((), (), s32[]{:S(2)}) async-start(), calls=%async_computation.12 | async-start | bytes 2621440 | tf_op jit(solution)/shard_map/all_gather | solution.py:187
  12.4 53.9 %copy-start.3 = (f32[512,2]{0,1:T(2,128)S(1)}, f32[512,2]{0,1:T(2,128)}, u32[]{:S(2)}) copy-start(f32[512,2]{0,1:T(2,128)} %param.22) | copy-start | bytes 12292
  12.4 61.8 %copy-start.1 = (bf16[2,256,2048]{2,1,0:T(8,128)(2,1)S(1)}, bf16[2,256,2048]{2,1,0:T(8,128)(2,1)}, u32[]{:S(2)}) copy-start(bf16[2,256,2048]{2,1,0:T(8,128)(2,1)} %param.25) | copy-start | bytes 6291460
  13.3 80.5 %copy-start.2 = (f32[2048]{0:T(1024)S(1)}, f32[2048]{0:T(1024)}, u32[]{:S(2)}) copy-start(f32[2048]{0:T(1024)} %param.14) | copy-start | bytes 24580
  67.6 18.9 %all-to-all-start.3 = ((f32[16,1,256]{2,1,0:T(1,128)}), f32[16,1,256]{2,1,0:T(1,128)S(1)}, u32[]{:S(2)}, u32[]{:S(2)}) async-start(f32[16,1,256]{2,1,0:T(1,128)} %all_to_all.32), calls=%async_computation.3 | async-start | bytes 32768 | tf_op jit(solution)/shard_map/all_to_all | solution.py:81
  74.2 68.7 %collective-permute-start.3 = (bf16[2,256,2048]{2,1,0:T(8,128)(2,1)S(1)}, bf16[2,256,2048]{2,1,0:T(8,128)(2,1)}, u32[]{:S(2)}, u32[]{:S(2)}) collective-permute-start(bf16[2,256,2048]{2,1,0:T(8,128)(2,1)S(1)} %copy-done.1), channel_id=1, source_target_pairs={{0,4},{4,0},{8,12},{12,8},{16,20},{20,16},{24,28},{28,24},{32,36},... | collective-permute-start | bytes 6291464 | tf_op jit(solution)/shard_map/ppermute | solution.py:166
  74.4 58.3 %collective-permute-start.1 = (bf16[2,2048,256]{2,1,0:T(8,128)(2,1)}, bf16[2,2048,256]{2,1,0:T(8,128)(2,1)}, u32[]{:S(2)}, u32[]{:S(2)}) collective-permute-start(bf16[2,2048,256]{2,1,0:T(8,128)(2,1)} %param.23), channel_id=1, source_target_pairs={{0,4},{4,0},{8,12},{12,8},{16,20},{20,16},{24,28},{28,24},{32,36},... | collective-permute-start | bytes 6291464 | tf_op jit(solution)/shard_map/ppermute | solution.py:166
  74.8 60.6 %collective-permute-start.2 = (bf16[2,2048,256]{2,1,0:T(8,128)(2,1)}, bf16[2,2048,256]{2,1,0:T(8,128)(2,1)}, u32[]{:S(2)}, u32[]{:S(2)}) collective-permute-start(bf16[2,2048,256]{2,1,0:T(8,128)(2,1)} %param.24), channel_id=1, source_target_pairs={{0,4},{4,0},{8,12},{12,8},{16,20},{20,16},{24,28},{28,24},{32,36},... | collective-permute-start | bytes 6291464 | tf_op jit(solution)/shard_map/ppermute | solution.py:166
  86.5 31.7 %all-to-all-start.2 = ((bf16[16,8,2048]{2,1,0:T(8,128)(2,1)}), bf16[16,8,2048]{2,1,0:T(8,128)(2,1)}, u32[]{:S(2)}, u32[]{:S(2)}) async-start(bf16[16,8,2048]{2,1,0:T(8,128)(2,1)} %get-tuple-element.2), calls=%async_computation.2 | async-start | bytes 1048576 | tf_op jit(solution)/shard_map/all_to_all | solution.py:81
  120.8 29.0 %all-to-all-start = ((bf16[4,128,2048]{2,1,0:T(8,128)(2,1)}), bf16[4,128,2048]{2,1,0:T(8,128)(2,1)}, u32[]{:S(2)}, u32[]{:S(2)}) async-start(bf16[4,128,2048]{2,1,0:T(8,128)(2,1)} %broadcast_in_dim.157), calls=%async_computation | async-start | bytes 4194304 | tf_op jit(solution)/shard_map/all_to_all | solution.py:22
  125.5 38.2 %all-gather.5.cloned.1.call-start = ((), (), s32[]{:S(2)}) async-start(), calls=%async_computation.11 | async-start | bytes 2621440 | tf_op jit(solution)/shard_map/all_gather | solution.py:187
  126.2 97.3 %reduce-scatter.5.cloned.1.call-start = ((), (), s32[]{:S(2)}) async-start(), calls=%async_computation.10 | async-start | bytes 2621440 | tf_op jit(solution)/shard_map/reduce_scatter | solution.py:196
  126.5 2.8 copy-start.4
  126.5 5.3 %copy-start.8 = (bf16[64,8,2048]{2,1,0:T(8,128)(2,1)S(1)}, bf16[64,8,2048]{2,1,0:T(8,128)(2,1)}, u32[]{:S(2)}) copy-start(bf16[64,8,2048]{2,1,0:T(8,128)(2,1)} %all-gather.7.cloned.1.call-done) | copy-start | bytes 6291460
  129.3 2.5 copy-start.6
  147.3 100.2 %reduce-scatter.3.cloned.1.call-start = ((), (), s32[]{:S(2)}) async-start(), calls=%async_computation.9 | async-start | bytes 2621440 | tf_op jit(solution)/shard_map/reduce_scatter | solution.py:196
  152.4 32.4 %collective-permute-start = (bf16[15,256]{1,0:T(8,128)(2,1)S(1)}, bf16[15,256]{1,0:T(8,128)(2,1)S(1)}, u32[]{:S(2)}, u32[]{:S(2)}) collective-permute-start(bf16[15,256]{1,0:T(8,128)(2,1)S(1)} %slice.168), channel_id=1, source_target_pairs={{0,4},{4,8},{8,12},{12,16},{16,20},{20,24},{24,28},{28,32},{32,36}... | collective-permute-start | bytes 23048 | tf_op jit(solution)/shard_map/ppermute | solution.py:17
  163.6 2.8 copy-start.5
  166.4 2.5 copy-start.9
  170.9 2.2 copy-start.7
  184.7 0.9 copy-start.10
  184.7 0.9 copy-start.11
  223.5 41.4 %all-to-all-start.6 = ((bf16[16,8,2048]{2,1,0:T(8,128)(2,1)}), bf16[16,8,2048]{2,1,0:T(8,128)(2,1)}, u32[]{:S(2)}, u32[]{:S(2)}) async-start(bf16[16,8,2048]{2,1,0:T(8,128)(2,1)} %bitcast.206), calls=%async_computation.8 | async-start | bytes 1048576 | tf_op jit(solution)/shard_map/all_to_all | solution.py:81
  264.8 35.5 %all-to-all-start.4 = ((bf16[16,8,2048]{2,1,0:T(8,128)(2,1)}), bf16[16,8,2048]{2,1,0:T(8,128)(2,1)}, u32[]{:S(2)}, u32[]{:S(2)}) async-start(bf16[16,8,2048]{2,1,0:T(8,128)(2,1)} %bitcast.207), calls=%async_computation.5 | async-start | bytes 1048576 | tf_op jit(solution)/shard_map/all_to_all | solution.py:81
Sparse Core Ops, SparseCore 0:
  66.4 32.6 all-gather.6
  128.1 35.5 all-gather.4
  166.2 42.4 reduce-scatter.4
  211.1 36.4 reduce-scatter.2
